TPU v7x, 32 devices: a whole 2x2x4 slice. The times are simulated.
32 devices in a mesh: grp: 2 (over y), ep: 4 (over z), tp: 4 (over x, core).
Axes of the slice: x: 2, y: 2, z: 4, core: 2. Of those that a mesh axis runs over, the one named last changes fastest.
Arguments:
- outer_gate: bfloat16 [4096, 1024], P(('grp', 'ep'), 'tp'), parts along dimension 0, may hold values from -6 to 6
- inner_gate: bfloat16 [4096, 1024], P(('grp', 'ep'), 'tp'), parts along dimension 0, may hold values from -6 to 6
- conv_input: bfloat16 [4096, 1024], P(('grp', 'ep'), 'tp'), parts along dimension 0, may hold values from -6 to 6
- conv_taps: float32 [3, 1024], P(None, 'tp'), may hold values from -3.5 to 3.5
- mixer_weight: bfloat16 [1024, 2048], P('tp'), may hold values from -0.1875 to 0.1875
- expert_input: bfloat16 [4096, 2048], P(('grp', 'ep', 'tp')), parts along dimension 0, may hold values from -6 to 6
- norm_gain: float32 [2048], replicated, may hold values from 0.1 to 1.9
- expert_ids: int32 [4096, 2], P(('grp', 'ep', 'tp')), parts along dimension 0, may hold values from 0 to 3, all different within a row; in each aligned block of 128 rows (0 to 127, 128 to 255, ...) at most 80 rows name the same one
- route_weight: float32 [4096, 2], P(('grp', 'ep', 'tp')), parts along dimension 0, may hold values from 0.25 to 1
- gate_weight: bfloat16 [4, 2048, 3072], P('ep', None, 'tp'), may hold values from -0.125 to 0.125
- up_weight: bfloat16 [4, 2048, 3072], P('ep', None, 'tp'), may hold values from -0.125 to 0.125
- down_weight: bfloat16 [4, 3072, 2048], P('ep', 'tp'), may hold values from -0.109375 to 0.109375
Outputs:
- mixer_output: bfloat16 [4096, 2048], P(('grp', 'ep', 'tp')), parts along dimension 0
- expert_output: bfloat16 [4096, 2048], P(('grp', 'ep', 'tp')), parts along dimension 0
There are 2 independent parts, one for each index of `grp`. A program takes and returns all parts, laid end to end along the dimension named above; an argument that names none is the same for every part. Nothing has to cross between parts.
Inputs may be any that keep to these rules, and one draw needn't show every extreme that they name: `expert_ids`: each row names 2 different experts. Among the rows of one device no expert is named more than 80 times, a bound that some block reaches.
All inputs are finite; a program needn't handle non-finite values.
Results may differ from a plain program's by a relative error of at most 0.011.
Values may be sent and summed in bfloat16 or wider, within the bound.
A program may use at most 128 MiB of HBM per device.

v0:
```python
import jax
import jax.numpy as jnp
from jax import lax
from jax.sharding import PartitionSpec as P

TAPS = 3


epsilon = 1e-06


def shifted(value, axis, steps):
    count = lax.axis_size(axis)
    initial, last = (max(0, -steps), min(count, count - steps))
    return lax.ppermute(value, axis, [(source, source + steps) for source in range(initial, last)])


def on_device(
    outer_gate,
    inner_gate,
    conv_input,
    conv_taps,
    mixer_weight,
    expert_input,
    norm_gain,
    expert_ids,
    route_weight,
    gate_weight,
    up_weight,
    down_weight,
):
    gated_rows = inner_gate.astype(jnp.float32) * conv_input.astype(jnp.float32)
    length = gated_rows.shape[0]
    earlier = shifted(gated_rows[length - (TAPS - 1) :], "ep", 1)
    padded = jnp.concatenate([earlier, gated_rows], axis=0)
    convolved = jnp.zeros_like(gated_rows)
    for tap_index in range(TAPS):
        convolved = convolved + conv_taps[tap_index] * padded[tap_index : tap_index + length]
    mixed = (outer_gate.astype(jnp.float32) * convolved).astype(jnp.bfloat16)
    mixer_output = lax.psum_scatter(
        jnp.dot(mixed, mixer_weight, preferred_element_type=jnp.float32).astype(jnp.bfloat16),
        "tp",
        scatter_dimension=0,
        tiled=True,
    )
    inputs = expert_input.astype(jnp.float32)
    normed = (
        inputs * lax.rsqrt(jnp.mean(inputs * inputs, axis=1, keepdims=True) + epsilon) * norm_gain
    ).astype(jnp.bfloat16)
    tokens_here, top_count = expert_ids.shape
    model_width = expert_input.shape[1]
    expert_count = lax.axis_size("ep") * gate_weight.shape[0]
    capacity = 5 * tokens_here * top_count // (4 * expert_count)
    flat_ids = expert_ids.reshape(-1)
    one_hot = (flat_ids[:, None] == jnp.arange(expert_count, dtype=jnp.int32)[None, :]).astype(
        jnp.int32
    )
    ranks = jnp.sum((jnp.cumsum(one_hot, axis=0) - 1) * one_hot, axis=1)
    target = flat_ids * capacity + ranks
    duplicates = jnp.broadcast_to(
        normed[:, None, :], (tokens_here, top_count, model_width)
    ).reshape(-1, model_width)
    outgoing = (
        jnp.zeros((expert_count * capacity, model_width), jnp.bfloat16).at[target].set(duplicates)
    )
    gate_local = gate_weight[0]
    up_local = up_weight[0]
    down_local = down_weight[0]
    arrived = lax.all_to_all(
        outgoing.reshape(expert_count, capacity, model_width),
        "ep",
        split_axis=0,
        concat_axis=0,
        tiled=True,
    )
    sources = arrived.shape[0]
    slot_count = arrived.shape[1]
    stacked = arrived.reshape(sources * slot_count, model_width)
    block_rows = lax.all_gather(stacked, "tp", axis=0, tiled=True)
    gate_value = jnp.dot(block_rows, gate_local, preferred_element_type=jnp.float32)
    up_value = jnp.dot(block_rows, up_local, preferred_element_type=jnp.float32)
    hidden = (jax.nn.silu(gate_value) * up_value).astype(jnp.bfloat16)
    own_sums = lax.psum_scatter(
        jnp.dot(hidden, down_local, preferred_element_type=jnp.float32).astype(jnp.bfloat16),
        "tp",
        scatter_dimension=0,
        tiled=True,
    )
    answers = lax.all_to_all(
        own_sums.reshape(sources, slot_count, model_width),
        "ep",
        split_axis=0,
        concat_axis=0,
        tiled=True,
    )
    picked = answers.reshape(expert_count * capacity, model_width)[target]
    picked = picked.astype(jnp.float32).reshape(tokens_here, top_count, model_width)
    expert_output = jnp.sum(picked * route_weight[:, :, None], axis=1).astype(jnp.bfloat16)
    return (mixer_output, expert_output)


def solution(mesh):
    return jax.shard_map(
        on_device,
        mesh=mesh,
        in_specs=(
            P(("grp", "ep"), "tp"),
            P(("grp", "ep"), "tp"),
            P(("grp", "ep"), "tp"),
            P(None, "tp"),
            P("tp", None),
            P(("grp", "ep", "tp"), None),
            P(),
            P(("grp", "ep", "tp"), None),
            P(("grp", "ep", "tp"), None),
            P("ep", None, "tp"),
            P("ep", None, "tp"),
            P("ep", "tp", None),
        ),
        out_specs=(P(("grp", "ep", "tp"), None), P(("grp", "ep", "tp"), None)),
        check_vma=False,
    )
```

profile of v0, /device:TPU:0, one launch (start us, length us, event | category | flops | bytes accessed | tf_op | source)
XLA Modules:
  0.0 224.8 jit_solution(13589981206200451405)
XLA Ops:
  7.2 0.9 copy.18
  8.4 0.7 broadcast_multiply_fusion
  9.1 1.2 reduce-window.6
  10.8 0.1 mul.102
  11.0 1.2 fusion.5
  12.2 1.2 fusion.7
  13.5 1.6 broadcast_in_dim.5
  15.1 2.3 %reshape.101 = bf16[256,2048]{1,0:T(8,128)(2,1)} reshape(bf16[128,2,2048]{2,1,0:T(2,128)(2,1)} %broadcast_in_dim.5) | data formatting | bytes 2097152 | tf_op jit(solution)/shard_map/reshape | solution.py:62
  17.4 4.0 %scatter_custom_fusion = bf16[320,2048]{1,0:T(8,128)(2,1)} fusion(s32[256]{0:T(256)S(1)} %bitcast.43, bf16[256,2048]{1,0:T(8,128)(2,1)} %reshape.101, bf16[]{:T(256)} %constant.9.clone.1), kind=kCustom, calls=%fused_computation.16 | custom fusion | bytes 1311232 | tf_op jit(solution)/shard_map/scatter | solution.py:64
  21.3 37.8 %all_to_all.10 = bf16[4,80,2048]{2,1,0:T(8,128)(2,1)} all-to-all(bf16[4,80,2048]{2,1,0:T(8,128)(2,1)} %bitcast.38), channel_id=1, replica_groups=mesh['grp'=2,'ep'=4,'tp'=4] {'ep'}, dimensions={0} | all-to-all | bytes 2621440 | tf_op jit(solution)/shard_map/all_to_all | solution.py:69
  59.2 39.7 %all-gather.2.cloned.1.call-done = bf16[1280,2048]{1,0:T(8,128)(2,1)} async-done(((bf16[320,2048]{1,0:T(8,128)(2,1)}), bf16[1280,2048]{1,0:T(8,128)(2,1)}) %all-gather.2.cloned.1.call-update) | async-done | bytes 5242896 | tf_op jit(solution)/shard_map/all_gather | solution.py:79
  98.9 7.2 %fusion.3 = f32[1280,768]{1,0:T(8,128)S(1)} fusion(bf16[1280,2048]{1,0:T(8,128)(2,1)} %all-gather.2.cloned.1.call-done, bf16[1,2048,768]{2,1,0:T(8,128)(2,1)} %param.21), kind=kOutput, calls=%fused_computation.7 | convolution fusion | flops 4026531840 | bytes 12320768 | tf_op jit(solution)/shard_map/dot_general | solution.py:80
  106.2 4.8 %fusion = bf16[1280,768]{1,0:T(8,128)(2,1)S(1)} fusion(bf16[1280,2048]{1,0:T(8,128)(2,1)S(1)} %copy-done.4, f32[1280,768]{1,0:T(8,128)S(1)} %fusion.3, bf16[1,2048,768]{2,1,0:T(8,128)(2,1)S(1)} %copy-done.5), kind=kOutput, calls=%fused_computation.4 | convolution fusion | flops 4032430080 | bytes 14286848 | tf_op jit(solution)/shard_map/dot_general | solution.py:81
  111.0 6.0 %convolution_convert_fusion = bf16[1280,2048]{1,0:T(8,128)(2,1)} fusion(bf16[1280,768]{1,0:T(8,128)(2,1)S(1)} %fusion, bf16[1,768,2048]{2,1,0:T(8,128)(2,1)S(1)} %copy-done), kind=kOutput, calls=%fused_computation.2 | convolution fusion | flops 4029153280 | bytes 10354688 | tf_op jit(solution)/shard_map/dot_general | solution.py:84
  117.1 1.1 convert_multiply_fusion.2
  118.2 3.6 %collective-permute-start = (f32[2,256]{1,0:T(2,128)S(1)}, f32[2,256]{1,0:T(2,128)S(1)}, u32[]{:S(2)}, u32[]{:S(2)}) collective-permute-start(f32[2,256]{1,0:T(2,128)S(1)} %slice.34), channel_id=1, source_target_pairs={{0,4},{4,8},{8,12},{1,5},{5,9},{9,13},{2,6},{6,10},{10,14},{3,7},{... | collective-permute-start | bytes 6152 | tf_op jit(solution)/shard_map/ppermute | solution.py:15
  121.8 1.1 collective-permute-done
  122.9 3.5 %convolution_convert_fusion.1 = bf16[512,2048]{1,0:T(8,128)(2,1)} fusion(bf16[256,2048]{1,0:T(8,128)(2,1)} %param.16, f32[2,256]{1,0:T(2,128)S(1)} %collective-permute-done, f32[512,256]{1,0:T(8,128)S(1)} %convert_multiply_fusion.2, bf16[512,256]{1,0:T(8,128)(2,1)S(1)} %copy-done.1, f32[256]{0:T(256)S(1)} %bitcast.41, f32[256]{0:T(256)S(1)} %bitcast.42, ...), kind=kOutput, calls=%fused_computation.9 | convolution fusion | flops 539230208 | bytes 3937280 | tf_op jit(solution)/shard_map/dot_general | solution.py:41
  126.5 42.0 %reduce-scatter.5.cloned.1.call-done = bf16[320,2048]{1,0:T(8,128)(2,1)} async-done(((bf16[1280,2048]{1,0:T(8,128)(2,1)}), bf16[320,2048]{1,0:T(8,128)(2,1)}) %reduce-scatter.5.cloned.1.call-update) | async-done | bytes 1310736 | tf_op jit(solution)/shard_map/reduce_scatter | solution.py:83
  168.5 4.6 %all-to-all-start.1 = ((bf16[4,80,2048]{2,1,0:T(8,128)(2,1)}), bf16[4,80,2048]{2,1,0:T(8,128)(2,1)}, u32[]{:S(2)}, u32[]{:S(2)}) async-start(bf16[4,80,2048]{2,1,0:T(8,128)(2,1)} %bitcast.39), calls=%async_computation.3 | async-start | bytes 2621440 | tf_op jit(solution)/shard_map/all_to_all | solution.py:89
  173.3 31.2 %all-to-all-done.1 = bf16[4,80,2048]{2,1,0:T(8,128)(2,1)} async-done(((bf16[4,80,2048]{2,1,0:T(8,128)(2,1)}), bf16[4,80,2048]{2,1,0:T(8,128)(2,1)}, u32[]{:S(2)}, u32[]{:S(2)}) %all-to-all-start.1) | async-done | bytes 1310752 | tf_op jit(solution)/shard_map/all_to_all | solution.py:89
  204.4 4.8 %gather_fusion = bf16[256,2048]{1,0:T(8,128)(2,1)} fusion(bf16[320,2048]{1,0:T(8,128)(2,1)} %bitcast.13, s32[1024]{0:T(1024)S(1)} %pad_clamp_fusion), kind=kCustom, calls=%fused_computation | custom fusion | bytes 2098176 | tf_op jit(solution)/shard_map/gather | solution.py:96
  209.3 3.4 %reshape.88 = f32[128,2,2048]{2,1,0:T(2,128)} reshape(bf16[256,2048]{1,0:T(8,128)(2,1)} %gather_fusion) | data formatting | bytes 3145728 | tf_op jit(solution)/shard_map/convert_element_type | solution.py:97
  212.7 5.6 %multiply_reduce_fusion = bf16[128,2048]{1,0:T(8,128)(2,1)} fusion(f32[128,2,2048]{2,1,0:T(2,128)} %reshape.88, f32[128,2]{1,0:T(8,128)S(1)} %copy.22), kind=kLoop, calls=%fused_computation.10 | loop fusion | flops 786432 | bytes 2622464 | tf_op jit(solution)/shard_map/reduce_sum | solution.py:98
  (36 shorter events, 1.1 us)
Async XLA Ops:
  7.2 103.8 %copy-start = (bf16[1,768,2048]{2,1,0:T(8,128)(2,1)S(1)}, bf16[1,768,2048]{2,1,0:T(8,128)(2,1)}, u32[]{:S(2)}) copy-start(bf16[1,768,2048]{2,1,0:T(8,128)(2,1)} %param.23) | copy-start | bytes 9437188
  7.2 91.7 %all-gather.2.cloned.1.call-start = ((), (), s32[]{:S(2)}) async-start(), calls=%async_computation.5 | async-start | bytes 6553600 | tf_op jit(solution)/shard_map/all_gather | solution.py:79
  59.2 109.4 %reduce-scatter.5.cloned.1.call-start = ((), (), s32[]{:S(2)}) async-start(), calls=%async_computation.6 | async-start | bytes 6553600 | tf_op jit(solution)/shard_map/reduce_scatter | solution.py:83
  98.9 7.3 %copy-start.4 = (bf16[1280,2048]{1,0:T(8,128)(2,1)S(1)}, bf16[1280,2048]{1,0:T(8,128)(2,1)}, u32[]{:S(2)}) copy-start(bf16[1280,2048]{1,0:T(8,128)(2,1)} %all-gather.2.cloned.1.call-done) | copy-start | bytes 15728644
  98.9 7.3 %copy-start.5 = (bf16[1,2048,768]{2,1,0:T(8,128)(2,1)S(1)}, bf16[1,2048,768]{2,1,0:T(8,128)(2,1)}, u32[]{:S(2)}) copy-start(bf16[1,2048,768]{2,1,0:T(8,128)(2,1)} %param.22) | copy-start | bytes 9437188
  117.0 4.8 %copy-start.2 = (f32[3,256]{1,0:T(4,128)S(1)}, f32[3,256]{1,0:T(4,128)}, u32[]{:S(2)}) copy-start(f32[3,256]{1,0:T(4,128)} %param.15) | copy-start | bytes 9220
  117.0 5.9 %copy-start.1 = (bf16[512,256]{1,0:T(8,128)(2,1)S(1)}, bf16[512,256]{1,0:T(8,128)(2,1)}, u32[]{:S(2)}) copy-start(bf16[512,256]{1,0:T(8,128)(2,1)} %param.12) | copy-start | bytes 786436
  117.0 101.2 %reduce-scatter.3.cloned.1.call-start = ((), (), s32[]{:S(2)}) async-start(), calls=%async_computation.4 | async-start | bytes 2621440 | tf_op jit(solution)/shard_map/reduce_scatter | solution.py:40
  118.2 4.7 %collective-permute-start = (f32[2,256]{1,0:T(2,128)S(1)}, f32[2,256]{1,0:T(2,128)S(1)}, u32[]{:S(2)}, u32[]{:S(2)}) collective-permute-start(f32[2,256]{1,0:T(2,128)S(1)} %slice.34), channel_id=1, source_target_pairs={{0,4},{4,8},{8,12},{1,5},{5,9},{9,13},{2,6},{6,10},{10,14},{3,7},{... | collective-permute-start | bytes 6152 | tf_op jit(solution)/shard_map/ppermute | solution.py:15
  126.5 46.7 %copy-start.3 = (f32[128,2]{0,1:T(2,128)S(1)}, f32[128,2]{0,1:T(2,128)}, u32[]{:S(2)}) copy-start(f32[128,2]{0,1:T(2,128)} %param.20) | copy-start | bytes 3076
  168.5 35.9 %all-to-all-start.1 = ((bf16[4,80,2048]{2,1,0:T(8,128)(2,1)}), bf16[4,80,2048]{2,1,0:T(8,128)(2,1)}, u32[]{:S(2)}, u32[]{:S(2)}) async-start(bf16[4,80,2048]{2,1,0:T(8,128)(2,1)} %bitcast.39), calls=%async_computation.3 | async-start | bytes 2621440 | tf_op jit(solution)/shard_map/all_to_all | solution.py:89
Sparse Core Ops, SparseCore 0:
  59.3 39.5 all-gather.1
  117.2 51.3 reduce-scatter.4
  171.6 31.1 reduce-scatter.2
where the time goes:
time: 225 us
  waiting for transfers between devices  114 us (51%)
  blocking collectives  37.8 us (17%)
  matrix products  21.6 us (10%)
  local copies, waits for them, and re-layouts  18 us (8%)
  between operations  13.9 us (6%)
  other arithmetic  11.2 us (5%)
  starting transfers between devices  8.28 us (4%)
    reduce_scatter x1, waiting for transfers between devices, on_device(): lax.psum_scatter(jnp.dot(hidden, down_local, preferred_element_type=jnp.f...  42 us
    all_gather x1, waiting for transfers between devices, on_device(): block_rows = lax.all_gather(stacked, 'tp', axis=0, tiled=True)  39.7 us
    all_to_all x1, blocking collectives, on_device(): lax.all_to_all(outgoing.reshape(expert_count, capacity, model_width), 'ep...  37.8 us
    all_to_all x1, waiting for transfers between devices, on_device(): lax.all_to_all(own_sums.reshape(sources, slot_count, model_width), 'ep',...  31.2 us
    dot_general x1, matrix products, on_device(): jnp.dot(block_rows, gate_local, preferred_element_type=jnp.float32)  7.24 us
    dot_general x1, matrix products, on_device(): jnp.dot(hidden, down_local, preferred_element_type=jnp.float32)  6.04 us
    reduce_sum x1, other arithmetic, on_device(): jnp.sum(picked * route_weight[:, :, None], axis=1).astype(jnp.bfloat16)  5.59 us
    gather x1, local copies, waits for them, and re-layouts, on_device(): picked = answers.reshape(expert_count * capacity, model_width)[target]  4.83 us
  transfers between devices with their start and end apart: 5, of which 4 were waited for; matrix products, arithmetic and copies ran while one was open for 8% of the time, Pallas kernels for 0%

commit v1 on v0

v1 whole, which is shorter than its diff:
```python
import functools

import jax
import jax.numpy as jnp
from jax import lax
from jax.experimental import pallas as pl
from jax.experimental.pallas import tpu as pltpu
from jax.sharding import PartitionSpec as P

EPSILON = 1e-06
F32 = jnp.float32
BF16 = jnp.bfloat16
MESH = pl.DeviceIdType.MESH
HALO = 8


def round_up(value, multiple):
    return (value + multiple - 1) // multiple * multiple


def add(*values):
    total = values[0].astype(F32)
    for value in values[1:]:
        total = total + value.astype(F32)
    return total.astype(BF16)


def kernel(
    n_ep,
    n_tp,
    cap,
    outer_ref,
    inner_ref,
    conv_ref,
    taps_ref,
    mixer_hbm,
    x_ref,
    gain_ref,
    ids_ref,
    ids_t_ref,
    route_ref,
    gate_hbm,
    up_hbm,
    down_hbm,
    mixer_out,
    expert_out,
    mixer_w,
    gate_w,
    up_w,
    down_w,
    normed,
    outbox,
    rows,
    part,
    core_in,
    chip_sum,
    cross_in,
    ret,
    ans,
    hid,
    gated,
    halo,
    mixed,
    m_part,
    m_core_in,
    m_chip_sum,
    m_cross_in,
    w_sem,
    z_send,
    z_recv,
    core_send,
    g_recv,
    cross_send,
    a_send,
    a_recv,
    b_send,
    b_recv,
    r_send,
    r_recv,
    h_sem,
    m_sem,
):
    half = n_tp // 2
    me = lax.axis_index("ep")
    t = lax.axis_index("tp")
    c = lax.rem(t, 2)
    a = t // 2
    pair = t + 1 - 2 * c
    others = [lax.rem(a + j, half) for j in range(1, half)]
    tokens, width = x_ref.shape
    length = inner_ref.shape[0]

    def source(i):
        if n_ep == 4:
            if i == 0:
                return me
            if i == 1:
                return me + 1 - 2 * lax.rem(me, 2)
            two = me + 2 - 4 * (me // 2)
            three = 3 - me
            inside = lax.rem((me + 1) // 2, 2)
            if i == 2:
                return two + inside * (three - two)
            return three + inside * (two - three)
        return lax.rem(me + i, n_ep)

    def remote(src, dst, send, recv, **where):
        return pltpu.make_async_remote_copy(
            src_ref=src,
            dst_ref=dst,
            send_sem=send,
            recv_sem=recv,
            device_id=where,
            device_id_type=MESH,
        )

    loads = [
        pltpu.make_async_copy(src, dst, w_sem.at[i])
        for i, (src, dst) in enumerate(
            [
                (mixer_hbm, mixer_w),
                (gate_hbm.at[0], gate_w),
                (up_hbm.at[0], up_w),
                (down_hbm.at[0], down_w),
            ]
        )
    ]
    for load in loads:
        load.start()

    barrier = pltpu.get_barrier_semaphore()
    for j in range(1, n_ep):
        pl.semaphore_signal(
            barrier, inc=1, device_id={"ep": lax.rem(me + j, n_ep)}, device_id_type=MESH
        )
    for j in range(1, n_tp):
        pl.semaphore_signal(
            barrier, inc=1, device_id={"tp": lax.rem(t + j, n_tp)}, device_id_type=MESH
        )

    values = x_ref[...].astype(F32)
    scale = lax.rsqrt(jnp.mean(values * values, axis=1, keepdims=True) + EPSILON)
    normed[...] = (values * scale * gain_ref[...]).astype(BF16)
    e_rows = round_up(n_ep, 8)
    e_iota = lax.broadcasted_iota(jnp.int32, (e_rows, tokens), 0)
    first, second = ids_t_ref[0:1, :], ids_t_ref[1:2, :]
    is_first, is_second = e_iota == first, e_iota == second
    named = jnp.where(is_first | is_second, 1.0, 0.0).astype(BF16)
    row_i = lax.broadcasted_iota(jnp.int32, (tokens, tokens), 0)
    col_i = lax.broadcasted_iota(jnp.int32, (tokens, tokens), 1)
    before = jnp.where(row_i < col_i, 1.0, 0.0).astype(BF16)
    rank = jnp.dot(named, before, preferred_element_type=F32)
    rank_1 = jnp.sum(jnp.where(is_first, rank, 0.0), axis=0, keepdims=True)
    rank_2 = jnp.sum(jnp.where(is_second, rank, 0.0), axis=0, keepdims=True)
    slot_1 = first.astype(F32) * cap + rank_1
    slot_2 = second.astype(F32) * cap + rank_2
    slots = lax.broadcasted_iota(jnp.int32, (n_ep * cap, tokens), 0).astype(F32)
    pack = jnp.where((slots == slot_1) | (slots == slot_2), 1.0, 0.0).astype(BF16)
    tile = 512
    for n in range(width // tile):
        cols = slice(n * tile, (n + 1) * tile)
        packed = jnp.dot(pack, normed[:, cols], preferred_element_type=F32)
        outbox[:, :, cols] = packed.astype(BF16).reshape(n_ep, cap, tile)

    gated[HALO:, :] = inner_ref[...].astype(F32) * conv_ref[...].astype(F32)

    pl.semaphore_wait(barrier, n_ep - 1 + n_tp - 1)

    nxt = lax.rem(me + 1, n_ep)
    halo_copy = remote(
        gated.at[pl.ds(length, HALO)], halo, h_sem.at[0], h_sem.at[1], ep=nxt
    )
    halo_copy.start()

    def dispatch(i):
        d = source(i)
        return remote(
            outbox.at[d], rows.at[me, t], z_send.at[d], z_recv.at[me], ep=d
        )

    def own_to_pair(s):
        return remote(
            rows.at[s, t], rows.at[s, t], core_send.at[s, t], g_recv.at[s, t], tp=pair
        )

    def own_to_cross(s, o):
        return remote(
            rows.at[s, t], rows.at[s, t], cross_send.at[s, o], g_recv.at[s, t], tp=2 * o + c
        )

    def cross_to_pair(s, o):
        q = 2 * o + c
        return remote(
            rows.at[s, q], rows.at[s, q], core_send.at[s, q], g_recv.at[s, q], tp=pair
        )

    def arrival(s, q):
        return remote(
            rows.at[s, q], rows.at[s, q], core_send.at[s, q], g_recv.at[s, q], tp=pair
        )

    def spread(s):
        for o in others:
            own_to_cross(s, o).start()
        own_to_pair(s).start()

    def pre(i):
        s = source(i)
        remote(outbox.at[s], rows.at[s, t], z_send.at[s], z_recv.at[s], ep=s).wait_recv()
        spread(s)

    def loop(lower, upper, body):
        if upper - lower <= 4:
            for i in range(lower, upper):
                body(i)
        else:
            lax.fori_loop(lower, upper, lambda i, _: (body(i), 0)[1], 0)

    rows[me, t] = outbox[me]
    spread(me)
    loop(1, n_ep, lambda i: dispatch(i).start())

    halo_copy.wait_recv()
    kept = jnp.where(me > 0, 1.0, 0.0)
    gated[0:HALO, :] = halo[...] * kept
    count = taps_ref.shape[0]
    convolved = jnp.zeros((length, gated.shape[1]), F32)
    for k in range(count):
        lower = HALO - (count - 1) + k
        convolved = convolved + taps_ref[k : k + 1, :] * gated[lower : lower + length, :]
    mixed[...] = (outer_ref[...].astype(F32) * convolved).astype(BF16)
    loads[0].wait()

    def mixer_tile(n, _):
        cols = pl.ds(pl.multiple_of(n * tile, tile), tile)
        for q in range(n_tp):
            value = jnp.dot(
                mixed[q * tokens : (q + 1) * tokens, :],
                mixer_w[:, cols],
                preferred_element_type=F32,
            )
            m_part[q % 2, q // 2, :, cols] = value.astype(BF16)
        return 0

    lax.fori_loop(0, width // tile, mixer_tile, 0)
    m_core = remote(m_part.at[1 - c], m_core_in, m_sem.at[0], m_sem.at[1], tp=pair)
    m_core.start()

    def m_cross(o):
        return remote(
            m_chip_sum.at[o],
            m_cross_in.at[a],
            m_sem.at[2 + o],
            m_sem.at[2 + half + a],
            tp=2 * o + c,
        )

    m_core.wait_recv()
    for o in others:
        m_chip_sum[o] = add(m_part[c, o], m_core_in[o])
        m_cross(o).start()

    def mixer_finish():
        for o in others:
            remote(
                m_chip_sum.at[o],
                m_cross_in.at[o],
                m_sem.at[2 + o],
                m_sem.at[2 + half + o],
                tp=2 * o + c,
            ).wait_recv()
        mixer_out[...] = add(
            m_part[c, a], m_core_in[a], *[m_cross_in[o] for o in others]
        )

    def gathered(i):
        s = source(i)
        for o in others:
            arrival(s, 2 * o + c).wait_recv()
            cross_to_pair(s, o).start()
        for o in range(half):
            arrival(s, 2 * o + 1 - c).wait_recv()

    f_tile = 256

    def compute(i):
        s = source(i)

        def up_tile(n, _):
            cols = pl.ds(pl.multiple_of(n * f_tile, f_tile), f_tile)
            block = rows[s].reshape(n_tp * cap, width)
            g = jnp.dot(block, gate_w[:, cols], preferred_element_type=F32)
            u = jnp.dot(block, up_w[:, cols], preferred_element_type=F32)
            hid[:, cols] = (g / (1.0 + jnp.exp(-g)) * u).astype(BF16)
            return 0

        lax.fori_loop(0, hid.shape[1] // f_tile, up_tile, 0)

        def down_tile(n, _):
            cols = pl.ds(pl.multiple_of(n * tile, tile), tile)
            value = jnp.dot(hid[...], down_w[:, cols], preferred_element_type=F32)
            value = value.astype(BF16).reshape(n_tp, cap, tile)
            for q in range(n_tp):
                part[s, q % 2, q // 2, :, cols] = value[q]
            return 0

        lax.fori_loop(0, width // tile, down_tile, 0)
        to_pair(s).start()

    def to_pair(s):
        return remote(
            part.at[s, 1 - c], core_in.at[s], a_send.at[s], a_recv.at[s], tp=pair
        )

    def to_cross(s, o):
        return remote(
            chip_sum.at[s, o], cross_in.at[s, a], b_send.at[s, o], b_recv.at[s, a], tp=2 * o + c
        )

    def middle(i):
        s = source(i)
        to_pair(s).wait_recv()
        for o in others:
            chip_sum[s, o] = add(part[s, c, o], core_in[s, o])
            to_cross(s, o).start()

    def give_back(s):
        return remote(ret.at[s], ans.at[me], r_send.at[s], r_recv.at[me], ep=s)

    def finish(i, own=False):
        s = source(i)
        for o in others:
            remote(
                chip_sum.at[s, o], cross_in.at[s, o], b_send.at[s, o], b_recv.at[s, o], tp=2 * o + c
            ).wait_recv()
        total = add(part[s, c, a], core_in[s, a], *[cross_in[s, o] for o in others])
        if own:
            ans[s] = total
        else:
            ret[s] = total
            give_back(s).start()

    def step(i):
        pre(i + 1)
        gathered(i)
        compute(i)
        finish(i - 1)
        middle(i)

    for load in loads[1:]:
        load.wait()
    pre(1)
    gathered(0)
    compute(0)
    middle(0)
    mixer_finish()
    pre(2)
    gathered(1)
    compute(1)
    finish(0, own=True)
    middle(1)
    loop(2, n_ep - 1, step)
    gathered(n_ep - 1)
    compute(n_ep - 1)
    finish(n_ep - 2)
    middle(n_ep - 1)
    finish(n_ep - 1)

    lanes = 128
    l_iota = lax.broadcasted_iota(jnp.int32, (tokens, lanes), 1)
    id_1, id_2 = ids_ref[:, 0:1], ids_ref[:, 1:2]
    l_first, l_second = l_iota == id_1, l_iota == id_2
    l_named = jnp.where(l_first | l_second, 1.0, 0.0).astype(BF16)
    after = jnp.where(col_i < row_i, 1.0, 0.0).astype(BF16)
    l_rank = jnp.dot(after, l_named, preferred_element_type=F32)
    p_1 = id_1.astype(F32) * cap + jnp.sum(
        jnp.where(l_first, l_rank, 0.0), axis=1, keepdims=True
    )
    p_2 = id_2.astype(F32) * cap + jnp.sum(
        jnp.where(l_second, l_rank, 0.0), axis=1, keepdims=True
    )
    places = lax.broadcasted_iota(jnp.int32, (tokens, n_ep * cap), 1).astype(F32)
    weight = jnp.where(places == p_1, route_ref[:, 0:1], 0.0) + jnp.where(
        places == p_2, route_ref[:, 1:2], 0.0
    )
    high = weight.astype(BF16)
    low = (weight - high.astype(F32)).astype(BF16)

    def answer_in(i):
        e = source(i)
        remote(ret.at[e], ans.at[e], r_send.at[e], r_recv.at[e], ep=e).wait_recv()

    loop(1, n_ep, answer_in)

    def combine_tile(n, _):
        cols = pl.ds(pl.multiple_of(n * tile, tile), tile)
        block = ans[:, :, cols].reshape(n_ep * cap, tile)
        expert_out[:, cols] = (
            jnp.dot(high, block, preferred_element_type=F32)
            + jnp.dot(low, block, preferred_element_type=F32)
        ).astype(BF16)
        return 0

    lax.fori_loop(0, width // tile, combine_tile, 0)

    halo_copy.wait_send()
    m_core.wait_send()
    for o in others:
        m_cross(o).wait_send()

    def drain(i):
        s = source(i)
        for o in others:
            own_to_cross(s, o).wait_send()
            cross_to_pair(s, o).wait_send()
            to_cross(s, o).wait_send()
        own_to_pair(s).wait_send()
        to_pair(s).wait_send()

    def drain_far(i):
        dispatch(i).wait_send()
        give_back(source(i)).wait_send()

    loop(0, n_ep, drain)
    loop(1, n_ep, drain_far)


def on_device(
    n_ep,
    n_tp,
    outer_gate,
    inner_gate,
    conv_input,
    conv_taps,
    mixer_weight,
    expert_input,
    norm_gain,
    expert_ids,
    route_weight,
    gate_weight,
    up_weight,
    down_weight,
):
    tokens, width = expert_input.shape
    top = expert_ids.shape[1]
    cap = round_up(5 * tokens * top // (4 * n_ep), 16)
    half = n_tp // 2
    length, channels = inner_gate.shape
    hidden = gate_weight.shape[2]
    vmem = pl.BlockSpec(memory_space=pltpu.VMEM)
    hbm = pl.BlockSpec(memory_space=pl.ANY)
    dma = pltpu.SemaphoreType.DMA
    v = pltpu.VMEM
    out = jax.ShapeDtypeStruct((tokens, width), BF16)
    return pl.pallas_call(
        functools.partial(kernel, n_ep, n_tp, cap),
        out_shape=(out, out),
        in_specs=[vmem] * 4 + [hbm] + [vmem] * 5 + [hbm] * 3,
        out_specs=(vmem, vmem),
        scratch_shapes=[
            v(mixer_weight.shape, BF16),
            v(gate_weight.shape[1:], BF16),
            v(up_weight.shape[1:], BF16),
            v(down_weight.shape[1:], BF16),
            v((tokens, width), BF16),
            v((n_ep, cap, width), BF16),
            v((n_ep, n_tp, cap, width), BF16),
            v((n_ep, 2, half, cap, width), BF16),
            v((n_ep, half, cap, width), BF16),
            v((n_ep, half, cap, width), BF16),
            v((n_ep, half, cap, width), BF16),
            v((n_ep, cap, width), BF16),
            v((n_ep, cap, width), BF16),
            v((n_tp * cap, hidden), BF16),
            v((HALO + length, channels), F32),
            v((HALO, channels), F32),
            v((length, channels), BF16),
            v((2, half, tokens, width), BF16),
            v((half, tokens, width), BF16),
            v((half, tokens, width), BF16),
            v((half, tokens, width), BF16),
            dma((4,)),
            dma((n_ep,)),
            dma((n_ep,)),
            dma((n_ep, n_tp)),
            dma((n_ep, n_tp)),
            dma((n_ep, half)),
            dma((n_ep,)),
            dma((n_ep,)),
            dma((n_ep, half)),
            dma((n_ep, half)),
            dma((n_ep,)),
            dma((n_ep,)),
            dma((2,)),
            dma((2 + 2 * half,)),
        ],
        compiler_params=pltpu.CompilerParams(
            collective_id=0, has_side_effects=True, vmem_limit_bytes=60 * 1024 * 1024
        ),
    )(
        outer_gate,
        inner_gate,
        conv_input,
        conv_taps,
        mixer_weight,
        expert_input,
        norm_gain.reshape(1, -1),
        expert_ids,
        expert_ids.T,
        route_weight,
        gate_weight,
        up_weight,
        down_weight,
    )


def solution(mesh):
    return jax.shard_map(
        functools.partial(on_device, mesh.shape["ep"], mesh.shape["tp"]),
        mesh=mesh,
        in_specs=(
            P(("grp", "ep"), "tp"),
            P(("grp", "ep"), "tp"),
            P(("grp", "ep"), "tp"),
            P(None, "tp"),
            P("tp", None),
            P(("grp", "ep", "tp"), None),
            P(),
            P(("grp", "ep", "tp"), None),
            P(("grp", "ep", "tp"), None),
            P("ep", None, "tp"),
            P("ep", None, "tp"),
            P("ep", "tp", None),
        ),
        out_specs=(P(("grp", "ep", "tp"), None), P(("grp", "ep", "tp"), None)),
        check_vma=False,
    )
```

time: 225 us -> 109 us (0.48)
  waiting for transfers between devices: 114 us -> 0 us
  Pallas kernels: 0 us -> 101 us
  blocking collectives: 37.8 us -> 0 us
  matrix products: 21.6 us -> 0 us
  between operations: 13.9 us -> 0.64 us
  local copies, waits for them, and re-layouts: 18 us -> 6.59 us
  other arithmetic: 11.2 us -> 0 us
  starting transfers between devices: 8.28 us -> 0 us
    pallas_call x0 -> x1, Pallas kernels: none -> 101 us  [on_device(): pl.pallas_call(functools.partial(kernel, n_ep, n_tp, cap), out_shape=(out...]
    reduce_scatter x2 -> x0, waiting for transfers between devices: 42.1 us -> none  [the longest x1 42 us: on_device(): lax.psum_scatter(jnp.dot(hidden, down_local, preferred_element_type=jnp.f...]
    all_gather x1 -> x0, waiting for transfers between devices: 39.7 us -> none  [on_device(): block_rows = lax.all_gather(stacked, 'tp', axis=0, tiled=True)]
    all_to_all x1 -> x0, blocking collectives: 37.8 us -> none  [on_device(): lax.all_to_all(outgoing.reshape(expert_count, capacity, model_width), 'ep...]
    all_to_all x1 -> x0, waiting for transfers between devices: 31.2 us -> none  [on_device(): lax.all_to_all(own_sums.reshape(sources, slot_count, model_width), 'ep',...]
    dot_general x4 -> x0, matrix products: 21.6 us -> none  [the longest x1 7.24 us: on_device(): jnp.dot(block_rows, gate_local, preferred_element_type=jnp.float32)]
    reduce_sum x3 -> x0, other arithmetic: 6.84 us -> none  [the longest x1 5.59 us: on_device(): jnp.sum(picked * route_weight[:, :, None], axis=1).astype(jnp.bfloat16)]
    unnamed x14 -> x4, local copies, waits for them, and re-layouts: 1.08 us -> 6.59 us
  transfers between devices with their start and end apart: 5 -> 0, of which waited for: 4 -> 0; matrix products, arithmetic and copies ran while one was open for 8% -> 0% of each run, Pallas kernels for 0% -> 0%
where the time goes in v1:
time: 109 us; the launch traced here: 108 us
  Pallas kernels  101 us (93%)
  local copies, waits for them, and re-layouts  6.59 us (6%)
    pallas_call x1, Pallas kernels, on_device(): pl.pallas_call(functools.partial(kernel, n_ep, n_tp, cap), out_shape=(out...  101 us
    unnamed x4, local copies, waits for them, and re-layouts  6.59 us

profile of v1, /device:TPU:0, one launch (start us, length us, event | category | flops | bytes accessed | tf_op | source)
XLA Modules:
  0.0 108.5 jit_solution(2372713802305364189)
XLA Ops:
  0.6 1.4 %copy.15.route_ref = f32[128,2]{1,0:T(8,128)} copy(f32[128,2]{0,1:T(2,128)} %param.20) | data formatting | bytes 2048 | tf_op args[8]
  2.0 1.4 %copy.14.ids_ref = s32[128,2]{1,0:T(8,128)} copy(s32[128,2]{0,1:T(2,128)} %param.19) | data formatting | bytes 2048 | tf_op args[7]
  3.5 101.2 %shard_map.131 = (bf16[128,2048]{1,0:T(8,128)(2,1)}, bf16[128,2048]{1,0:T(8,128)(2,1)}) custom-call(bf16[512,256]{1,0:T(8,128)(2,1)} %outer_ref.1, bf16[512,256]{1,0:T(8,128)(2,1)} %inner_ref.1, bf16[512,256]{1,0:T(8,128)(2,1)} %conv_ref.1, f32[3,256]{1,0:T(4,128)} %taps_ref.1, bf16[256,2048]{1,0:T(8,128)(2,1)} %mixer_hbm.1, bf16[128,2048]{1,0:T(8,128)(2,1)} %x_ref.1, ...), custom_call_target="tpu_custom_call" | custom-call | tf_op jit(solution)/shard_map/pallas_call | solution.py:455
  104.7 1.9 %copy.18 = bf16[128,2048]{1,0:T(8,128)(2,1)} copy(bf16[128,2048]{1,0:T(8,128)(2,1)} %get-tuple-element.4) | data formatting | bytes 1048576
  106.6 1.9 %copy.19 = bf16[128,2048]{1,0:T(8,128)(2,1)} copy(bf16[128,2048]{1,0:T(8,128)(2,1)} %get-tuple-element.5) | data formatting | bytes 1048576

commit v2 on v1

--- a/solution.py
+++ b/solution.py
@@ -37,7 +37,6 @@
     x_ref,
     gain_ref,
     ids_ref,
-    ids_t_ref,
     route_ref,
     gate_hbm,
     up_hbm,
@@ -49,6 +48,7 @@
     up_w,
     down_w,
     normed,
+    weights,
     outbox,
     rows,
     part,
@@ -90,18 +90,29 @@
     tokens, width = x_ref.shape
     length = inner_ref.shape[0]
 
-    def source(i):
+    def departure(i):
         if n_ep == 4:
             if i == 0:
                 return me
+            two = me + 2 - 4 * (me // 2)
             if i == 1:
-                return me + 1 - 2 * lax.rem(me, 2)
-            two = me + 2 - 4 * (me // 2)
+                return two
+            one = me + 1 - 2 * lax.rem(me, 2)
             three = 3 - me
             inside = lax.rem((me + 1) // 2, 2)
             if i == 2:
-                return two + inside * (three - two)
-            return three + inside * (two - three)
+                return one + inside * (three - one)
+            return three + inside * (one - three)
+        return lax.rem(me + i, n_ep)
+
+    def source(i):
+        if n_ep == 4:
+            return [
+                me,
+                me + 2 - 4 * (me // 2),
+                3 - me,
+                me + 1 - 2 * lax.rem(me, 2),
+            ][i]
         return lax.rem(me + i, n_ep)
 
     def remote(src, dst, send, recv, **where):
@@ -143,7 +154,7 @@
     normed[...] = (values * scale * gain_ref[...]).astype(BF16)
     e_rows = round_up(n_ep, 8)
     e_iota = lax.broadcasted_iota(jnp.int32, (e_rows, tokens), 0)
-    first, second = ids_t_ref[0:1, :], ids_t_ref[1:2, :]
+    first, second = ids_ref[0:1, :], ids_ref[1:2, :]
     is_first, is_second = e_iota == first, e_iota == second
     named = jnp.where(is_first | is_second, 1.0, 0.0).astype(BF16)
     row_i = lax.broadcasted_iota(jnp.int32, (tokens, tokens), 0)
@@ -173,7 +184,7 @@
     halo_copy.start()
 
     def dispatch(i):
-        d = source(i)
+        d = departure(i)
         return remote(
             outbox.at[d], rows.at[me, t], z_send.at[d], z_recv.at[me], ep=d
         )
@@ -246,29 +257,30 @@
     m_core = remote(m_part.at[1 - c], m_core_in, m_sem.at[0], m_sem.at[1], tp=pair)
     m_core.start()
 
-    def m_cross(o):
-        return remote(
-            m_chip_sum.at[o],
-            m_cross_in.at[a],
-            m_sem.at[2 + o],
-            m_sem.at[2 + half + a],
+    piece = tokens // 2
+
+    def m_cross(o, h, slot):
+        return remote(
+            m_chip_sum.at[o, pl.ds(h * piece, piece)],
+            m_cross_in.at[slot, pl.ds(h * piece, piece)],
+            m_sem.at[2 + 2 * o + h],
+            m_sem.at[2 + n_tp + 2 * slot + h],
             tp=2 * o + c,
         )
 
     m_core.wait_recv()
     for o in others:
         m_chip_sum[o] = add(m_part[c, o], m_core_in[o])
-        m_cross(o).start()
+        m_cross(o, 0, a).start()
+
+    def mixer_rest():
+        for o in others:
+            m_cross(o, 1, a).start()
 
     def mixer_finish():
         for o in others:
-            remote(
-                m_chip_sum.at[o],
-                m_cross_in.at[o],
-                m_sem.at[2 + o],
-                m_sem.at[2 + half + o],
-                tp=2 * o + c,
-            ).wait_recv()
+            m_cross(o, 0, o).wait_recv()
+            m_cross(o, 1, o).wait_recv()
         mixer_out[...] = add(
             m_part[c, a], m_core_in[a], *[m_cross_in[o] for o in others]
         )
@@ -350,54 +362,45 @@
     for load in loads[1:]:
         load.wait()
     pre(1)
+    mixer_rest()
     gathered(0)
     compute(0)
-    middle(0)
-    mixer_finish()
     pre(2)
     gathered(1)
     compute(1)
-    finish(0, own=True)
     middle(1)
     loop(2, n_ep - 1, step)
     gathered(n_ep - 1)
     compute(n_ep - 1)
     finish(n_ep - 2)
     middle(n_ep - 1)
+    middle(0)
+    mixer_finish()
+
+    weight = jnp.where(slots == slot_1, route_ref[0:1, :], 0.0) + jnp.where(
+        slots == slot_2, route_ref[1:2, :], 0.0
+    )
+    weights[0] = weight.astype(BF16)
+    weights[1] = (weight - weight.astype(BF16).astype(F32)).astype(BF16)
     finish(n_ep - 1)
-
-    lanes = 128
-    l_iota = lax.broadcasted_iota(jnp.int32, (tokens, lanes), 1)
-    id_1, id_2 = ids_ref[:, 0:1], ids_ref[:, 1:2]
-    l_first, l_second = l_iota == id_1, l_iota == id_2
-    l_named = jnp.where(l_first | l_second, 1.0, 0.0).astype(BF16)
-    after = jnp.where(col_i < row_i, 1.0, 0.0).astype(BF16)
-    l_rank = jnp.dot(after, l_named, preferred_element_type=F32)
-    p_1 = id_1.astype(F32) * cap + jnp.sum(
-        jnp.where(l_first, l_rank, 0.0), axis=1, keepdims=True
-    )
-    p_2 = id_2.astype(F32) * cap + jnp.sum(
-        jnp.where(l_second, l_rank, 0.0), axis=1, keepdims=True
-    )
-    places = lax.broadcasted_iota(jnp.int32, (tokens, n_ep * cap), 1).astype(F32)
-    weight = jnp.where(places == p_1, route_ref[:, 0:1], 0.0) + jnp.where(
-        places == p_2, route_ref[:, 1:2], 0.0
-    )
-    high = weight.astype(BF16)
-    low = (weight - high.astype(F32)).astype(BF16)
+    finish(0, own=True)
 
     def answer_in(i):
         e = source(i)
         remote(ret.at[e], ans.at[e], r_send.at[e], r_recv.at[e], ep=e).wait_recv()
 
     loop(1, n_ep, answer_in)
+
+    def weighted(left, right):
+        return lax.dot_general(
+            left, right, (((0,), (0,)), ((), ())), preferred_element_type=F32
+        )
 
     def combine_tile(n, _):
         cols = pl.ds(pl.multiple_of(n * tile, tile), tile)
         block = ans[:, :, cols].reshape(n_ep * cap, tile)
         expert_out[:, cols] = (
-            jnp.dot(high, block, preferred_element_type=F32)
-            + jnp.dot(low, block, preferred_element_type=F32)
+            weighted(weights[0], block) + weighted(weights[1], block)
         ).astype(BF16)
         return 0
 
@@ -406,7 +409,8 @@
     halo_copy.wait_send()
     m_core.wait_send()
     for o in others:
-        m_cross(o).wait_send()
+        m_cross(o, 0, a).wait_send()
+        m_cross(o, 1, a).wait_send()
 
     def drain(i):
         s = source(i)
@@ -455,7 +459,7 @@
     return pl.pallas_call(
         functools.partial(kernel, n_ep, n_tp, cap),
         out_shape=(out, out),
-        in_specs=[vmem] * 4 + [hbm] + [vmem] * 5 + [hbm] * 3,
+        in_specs=[vmem] * 4 + [hbm] + [vmem] * 4 + [hbm] * 3,
         out_specs=(vmem, vmem),
         scratch_shapes=[
             v(mixer_weight.shape, BF16),
@@ -463,6 +467,7 @@
             v(up_weight.shape[1:], BF16),
             v(down_weight.shape[1:], BF16),
             v((tokens, width), BF16),
+            v((2, n_ep * cap, tokens), BF16),
             v((n_ep, cap, width), BF16),
             v((n_ep, n_tp, cap, width), BF16),
             v((n_ep, 2, half, cap, width), BF16),
@@ -492,7 +497,7 @@
             dma((n_ep,)),
             dma((n_ep,)),
             dma((2,)),
-            dma((2 + 2 * half,)),
+            dma((2 + 2 * n_tp,)),
         ],
         compiler_params=pltpu.CompilerParams(
             collective_id=0, has_side_effects=True, vmem_limit_bytes=60 * 1024 * 1024
@@ -505,9 +510,8 @@
         mixer_weight,
         expert_input,
         norm_gain.reshape(1, -1),
-        expert_ids,
         expert_ids.T,
-        route_weight,
+        route_weight.T,
         gate_weight,
         up_weight,
         down_weight,

time: 109 us -> 92.6 us (0.85)
  Pallas kernels: 101 us -> 87.9 us
  local copies, waits for them, and re-layouts: 6.59 us -> 3.76 us
    pallas_call x1, Pallas kernels: 101 us -> 87.9 us  [on_device(): pl.pallas_call(functools.partial(kernel, n_ep, n_tp, cap), out_shape=(out...]
    unnamed x4 -> x2, local copies, waits for them, and re-layouts: 6.59 us -> 3.76 us
where the time goes in v2:
time: 92.6 us; the launch traced here: 92.3 us
  Pallas kernels  87.9 us (95%)
  local copies, waits for them, and re-layouts  3.76 us (4%)
    pallas_call x1, Pallas kernels, on_device(): pl.pallas_call(functools.partial(kernel, n_ep, n_tp, cap), out_shape=(out...  87.9 us
    unnamed x2, local copies, waits for them, and re-layouts  3.76 us

profile of v2, /device:TPU:0, one launch (start us, length us, event | category | flops | bytes accessed | tf_op | source)
XLA Modules:
  0.0 92.3 jit_solution(15324310580644594639)
XLA Ops:
  0.6 87.9 %shard_map.131 = (bf16[128,2048]{1,0:T(8,128)(2,1)}, bf16[128,2048]{1,0:T(8,128)(2,1)}) custom-call(bf16[512,256]{1,0:T(8,128)(2,1)} %outer_ref.1, bf16[512,256]{1,0:T(8,128)(2,1)} %inner_ref.1, bf16[512,256]{1,0:T(8,128)(2,1)} %conv_ref.1, f32[3,256]{1,0:T(4,128)} %taps_ref.1, bf16[256,2048]{1,0:T(8,128)(2,1)} %mixer_hbm.1, bf16[128,2048]{1,0:T(8,128)(2,1)} %x_ref.1, ...), custom_call_target="tpu_custom_call" | custom-call | tf_op jit(solution)/shard_map/pallas_call | solution.py:459
  88.6 1.9 %copy.16 = bf16[128,2048]{1,0:T(8,128)(2,1)} copy(bf16[128,2048]{1,0:T(8,128)(2,1)} %get-tuple-element.4) | data formatting | bytes 1048576
  90.5 1.9 %copy.17 = bf16[128,2048]{1,0:T(8,128)(2,1)} copy(bf16[128,2048]{1,0:T(8,128)(2,1)} %get-tuple-element.5) | data formatting | bytes 1048576

commit v3 on v2

--- a/solution.py
+++ b/solution.py
@@ -107,12 +107,10 @@
 
     def source(i):
         if n_ep == 4:
-            return [
-                me,
-                me + 2 - 4 * (me // 2),
-                3 - me,
-                me + 1 - 2 * lax.rem(me, 2),
-            ][i]
+            one = me + 1 - 2 * lax.rem(me, 2)
+            inside = lax.rem((me + 1) // 2, 2)
+            later = inside * (3 - me - one)
+            return [me, me + 2 - 4 * (me // 2), 3 - me - later, one + later][i]
         return lax.rem(me + i, n_ep)
 
     def remote(src, dst, send, recv, **where):
@@ -361,8 +359,8 @@
 
     for load in loads[1:]:
         load.wait()
+    mixer_rest()
     pre(1)
-    mixer_rest()
     gathered(0)
     compute(0)
     pre(2)

time: 92.6 us -> 93.6 us (1.011)
  the two profiles are of different devices: /device:TPU:0 before, /device:TPU:9 now
where the time goes in v3:
time: 93.6 us; the launch traced here: 93.3 us
  Pallas kernels  88.9 us (95%)
  local copies, waits for them, and re-layouts  3.76 us (4%)
    pallas_call x1, Pallas kernels, on_device(): pl.pallas_call(functools.partial(kernel, n_ep, n_tp, cap), out_shape=(out...  88.9 us
    unnamed x2, local copies, waits for them, and re-layouts  3.76 us

profile of v3, /device:TPU:9, one launch (start us, length us, event | category | flops | bytes accessed | tf_op | source)
XLA Modules:
  0.0 93.3 jit_solution(11740061807335395069)
XLA Ops:
  0.6 88.9 %shard_map.131 = (bf16[128,2048]{1,0:T(8,128)(2,1)}, bf16[128,2048]{1,0:T(8,128)(2,1)}) custom-call(bf16[512,256]{1,0:T(8,128)(2,1)} %outer_ref.1, bf16[512,256]{1,0:T(8,128)(2,1)} %inner_ref.1, bf16[512,256]{1,0:T(8,128)(2,1)} %conv_ref.1, f32[3,256]{1,0:T(4,128)} %taps_ref.1, bf16[256,2048]{1,0:T(8,128)(2,1)} %mixer_hbm.1, bf16[128,2048]{1,0:T(8,128)(2,1)} %x_ref.1, ...), custom_call_target="tpu_custom_call" | custom-call | tf_op jit(solution)/shard_map/pallas_call | solution.py:457
  89.6 1.9 %copy.16 = bf16[128,2048]{1,0:T(8,128)(2,1)} copy(bf16[128,2048]{1,0:T(8,128)(2,1)} %get-tuple-element.4) | data formatting | bytes 1048576
  91.5 1.9 %copy.17 = bf16[128,2048]{1,0:T(8,128)(2,1)} copy(bf16[128,2048]{1,0:T(8,128)(2,1)} %get-tuple-element.5) | data formatting | bytes 1048576
